TPU v7x, 32 devices: a whole 2x2x4 slice. The times are simulated.
32 devices in a mesh: grp: 2 (over y), dp: 2 (over x), kv: 4 (over z), tp: 2 (over core).
Axes of the slice: x: 2, y: 2, z: 4, core: 2. Of those that a mesh axis runs over, the one named last changes fastest.
Arguments:
- tokens: bfloat16 [32, 2048], P(('grp', 'dp'), ('kv', 'tp')), parts along dimension 0, may hold values from -40 to 40
- past_state: float32 [32, 16, 128, 128], P(('grp', 'dp', 'kv'), 'tp'), parts along dimension 0, may hold values from -4 to 4
- mix_gain: float32 [2048], P('kv'), may hold values from 0.1 to 1.9
- w_query: bfloat16 [2048, 2048], P('kv', 'tp'), may hold values from -0.125 to 0.125
- w_forget: bfloat16 [2048, 2048], P('kv', 'tp'), may hold values from -0.125 to 0.125
- w_value: bfloat16 [2048, 2048], P('kv', 'tp'), may hold values from -0.125 to 0.125
- w_gate_out: bfloat16 [2048, 2048], P('kv', 'tp'), may hold values from -0.125 to 0.125
- floor_logits: float32 [2048], P('tp'), may hold values from -6 to 6
- head_gain: float32 [128], replicated, may hold values from 0.1 to 1.9
- w_out: bfloat16 [2048, 2048], P(None, ('kv', 'tp')), may hold values from -0.125 to 0.125
- mlp_gain: float32 [2048], replicated, may hold values from 0.1 to 1.9
- w_gate: bfloat16 [2048, 5632], P(None, ('kv', 'tp')), may hold values from -0.125 to 0.125
- w_up: bfloat16 [2048, 5632], P(None, ('kv', 'tp')), may hold values from -0.125 to 0.125
- w_down: bfloat16 [5632, 2048], P(('kv', 'tp')), may hold values from -0.109375 to 0.109375
Outputs:
- result: bfloat16 [32, 2048], P(('grp', 'dp'), ('kv', 'tp')), parts along dimension 0
- new_state: float32 [32, 16, 128, 128], P(('grp', 'dp', 'kv'), 'tp'), parts along dimension 0
There are 2 independent parts, one for each index of `grp`. A program takes and returns all parts, laid end to end along the dimension named above; an argument that names none is the same for every part. Nothing has to cross between parts.
All inputs are finite; a program needn't handle non-finite values.
Results may differ from a plain program's by a relative error of at most 0.0091.
Values may be sent and summed in bfloat16 or wider, within the bound.
A program may use at most 64 MiB of HBM per device.

v0:
```python
import jax
import jax.numpy as jnp
from jax import lax
from jax.sharding import PartitionSpec as P

D = 2048
DK = 128
DV = 128
epsilon = 1e-06


def body(
    tokens,
    past_state,
    mix_gain,
    w_query,
    w_forget,
    w_value,
    w_gate_out,
    floor_logits,
    head_gain,
    w_out,
    mlp_gain,
    w_gate,
    w_up,
    w_down,
):
    kv_count = lax.axis_size("kv")
    tp_count = lax.axis_size("tp")
    rows_local = past_state.shape[0]
    heads_local = past_state.shape[1]
    width_cols = tokens.shape[1]
    own_block = lax.all_gather(tokens, "tp", axis=1, tiled=True)
    block_f = own_block.astype(jnp.float32)
    square_rows = lax.psum(jnp.sum(block_f * block_f, axis=1), "kv")
    gained = (own_block.astype(jnp.float32) * mix_gain).astype(jnp.bfloat16)
    mine = lax.dynamic_slice_in_dim(square_rows, lax.axis_index("kv") * rows_local, rows_local, 0)
    row_scale = lax.rsqrt(mine / D + epsilon)[:, None]
    query_sum, forget_sum, value_sum, gate_sum = (
        lax.psum_scatter(
            jnp.dot(gained, w_query, preferred_element_type=jnp.float32),
            "kv",
            scatter_dimension=0,
            tiled=True,
        ),
        lax.psum_scatter(
            jnp.dot(gained, w_forget, preferred_element_type=jnp.float32),
            "kv",
            scatter_dimension=0,
            tiled=True,
        ),
        lax.psum_scatter(
            jnp.dot(gained, w_value, preferred_element_type=jnp.float32),
            "kv",
            scatter_dimension=0,
            tiled=True,
        ),
        lax.psum_scatter(
            jnp.dot(gained, w_gate_out, preferred_element_type=jnp.float32),
            "kv",
            scatter_dimension=0,
            tiled=True,
        ),
    )
    query = query_sum * row_scale
    forget_pre = forget_sum * row_scale
    value = value_sum * row_scale
    gate_pre = gate_sum * row_scale
    lower = jax.nn.sigmoid(floor_logits).reshape(heads_local, DK)
    forget = lower + (1.0 - lower) * jax.nn.sigmoid(forget_pre.reshape(rows_local, heads_local, DK))
    values = value.reshape(rows_local, heads_local, DV)
    new_state = forget[..., None] * past_state + (1.0 - forget)[..., None] * values[:, :, None, :]
    activ = jax.nn.silu(query.reshape(rows_local, heads_local, DK))
    head_out = jnp.einsum("shkv,shk->shv", new_state, activ, precision=lax.Precision.HIGHEST)
    normed = head_out * lax.rsqrt(jnp.mean(head_out * head_out, axis=2, keepdims=True) + epsilon)
    normed = normed * head_gain * jax.nn.silu(gate_pre.reshape(rows_local, heads_local, DV))
    mixed = normed.reshape(1, rows_local, heads_local * DV).astype(jnp.bfloat16)
    every_head = lax.all_gather(mixed, ("kv", "tp"), axis=0, tiled=True)
    every_head = every_head.reshape(kv_count, tp_count, rows_local, heads_local * DV)
    out_blocks = w_out.reshape(tp_count, heads_local * DV, width_cols)
    projected = jnp.einsum(
        "ktsh,thc->ksc", every_head, out_blocks, preferred_element_type=jnp.float32
    )
    middle = (
        tokens.astype(jnp.float32) + projected.reshape(kv_count * rows_local, width_cols)
    ).astype(jnp.bfloat16)
    gathered = lax.all_gather(middle, ("kv", "tp"), axis=1, tiled=True)
    gathered_f = gathered.astype(jnp.float32)
    mlp_scale = lax.rsqrt(jnp.mean(gathered_f * gathered_f, axis=1, keepdims=True) + epsilon)
    mlp_in = (gathered_f * mlp_scale * mlp_gain).astype(jnp.bfloat16)
    gate = jnp.dot(mlp_in, w_gate, preferred_element_type=jnp.float32)
    upward = jnp.dot(mlp_in, w_up, preferred_element_type=jnp.float32)
    hidden = (jax.nn.silu(gate) * upward).astype(jnp.bfloat16)
    terms = jnp.dot(hidden, w_down, preferred_element_type=jnp.float32)
    summed = lax.psum_scatter(terms, ("kv", "tp"), scatter_dimension=1, tiled=True)
    result = (middle.astype(jnp.float32) + summed).astype(jnp.bfloat16)
    return (result, new_state)


def solution(mesh):
    placed = (
        P(("grp", "dp"), ("kv", "tp")),
        P(("grp", "dp", "kv"), "tp", None, None),
        P("kv"),
        P("kv", "tp"),
        P("kv", "tp"),
        P("kv", "tp"),
        P("kv", "tp"),
        P("tp"),
        P(),
        P(None, ("kv", "tp")),
        P(),
        P(None, ("kv", "tp")),
        P(None, ("kv", "tp")),
        P(("kv", "tp"), None),
    )
    return jax.shard_map(
        body,
        mesh=mesh,
        in_specs=placed,
        out_specs=(P(("grp", "dp"), ("kv", "tp")), P(("grp", "dp", "kv"), "tp", None, None)),
        check_vma=False,
    )
```

profile of v0, /device:TPU:0, one launch (start us, length us, event | category | flops | bytes accessed | tf_op | source)
XLA Modules:
  0.0 136.3 jit_solution(9865820180472469167)
XLA Ops:
  7.3 2.2 %all_gather.9 = bf16[8,512]{1,0:T(8,128)(2,1)S(1)} all-gather(bf16[8,256]{1,0:T(8,128)(2,1)} %param.14), channel_id=1, replica_groups=mesh['grp'=2,'dp'=2,'kv'=4,'tp'=2] {'tp'}, dimensions={1}, use_global_device_ids=true | all-gather | bytes 12288 | tf_op jit(solution)/shard_map/all_gather | solution.py:33
  9.5 0.6 fusion.13
  10.1 2.1 %fusion.38 = f32[8,1024]{1,0:T(8,128)} fusion(bf16[512,1024]{1,0:T(8,128)(2,1)} %param.19, bf16[8,512]{1,0:T(8,128)(2,1)S(1)} %all_gather.9, f32[512]{0:T(512)} %param.16), kind=kOutput, calls=%fused_computation.55 | convolution fusion | flops 8400896 | bytes 1091584 | tf_op jit(solution)/shard_map/dot_general | solution.py:53
  12.2 2.1 %fusion.36 = f32[8,1024]{1,0:T(8,128)} fusion(bf16[512,1024]{1,0:T(8,128)(2,1)} %param.17, bf16[8,512]{1,0:T(8,128)(2,1)S(1)} %all_gather.9, f32[512]{0:T(512)} %param.16), kind=kOutput, calls=%fused_computation.54 | convolution fusion | flops 8400896 | bytes 1091584 | tf_op jit(solution)/shard_map/dot_general | solution.py:41
  14.3 2.1 %fusion.34 = f32[8,1024]{1,0:T(8,128)} fusion(bf16[512,1024]{1,0:T(8,128)(2,1)} %param.20, bf16[8,512]{1,0:T(8,128)(2,1)S(1)} %all_gather.9, f32[512]{0:T(512)} %param.16), kind=kOutput, calls=%fused_computation.53 | convolution fusion | flops 8400896 | bytes 1091584 | tf_op jit(solution)/shard_map/dot_general | solution.py:59
  16.5 0.9 fusion.40
  17.4 0.0 reduce-scatter.2.cloned.1.call-start
  17.5 0.7 dynamic-slice
  18.8 36.2 %all-reduce.7.cloned.1.call-done = (f32[8,1024]{1,0:T(8,128)}, f32[8]{0:T(128)}, f32[8,1024]{1,0:T(8,128)}, f32[8,1024]{1,0:T(8,128)}, f32[8,1024]{1,0:T(8,128)}) async-done(((f32[8,1024]{1,0:T(8,128)}, f32[8]{0:T(128)}, f32[8,1024]{1,0:T(8,128)}, f32[8,1024]{1,0:T(8,128)}, f32[8,1024]{1,0:T(8,128)}), (f32[8,1024]{1,0:T(8,128)}, f32[8]{0:T(128)}, f32[8,1024]{1,0:T(8,128)}, f32[8,1024]{1,0:T(8,128)}, ...) | async-done | bytes 131120
  55.1 0.8 add_rsqrt_fusion.2
  55.8 0.9 fusion.24
  56.8 1.8 %multiply_add_fusion = f32[2,8,128,128]{3,2,1,0:T(8,128)S(1)} fusion(f32[2,8,128,128]{3,2,1,0:T(8,128)} %param.15, f32[2,8,128]{2,1,0:T(8,128)S(1)} %bitcast.79, f32[2,8,128]{2,1,0:T(8,128)S(1)} %get-tuple-element.7, f32[2,8,128]{2,1,0:T(8,128)S(1)} %get-tuple-element.8), kind=kLoop, calls=%fused_computation.6 | loop fusion | flops 786432 | bytes 2121728 | tf_op jit(solution)/shard_map/add | solution.py:72
  58.6 1.0 copy-done.1
  59.6 1.0 fusion.44
  60.6 0.1 multiply_reduce_fusion
  60.7 0.1 fusion.29
  60.8 14.1 %all_gather.10 = bf16[8,2,1024]{2,1,0:T(2,128)(2,1)S(1)} all-gather(bf16[1,2,1024]{2,1,0:T(2,128)(2,1)S(1)} %convert_element_type.46), channel_id=1, replica_groups=mesh['grp'=2,'dp'=2,'kv'=4,'tp'=2] {'kv','tp'}, dimensions={0}, use_global_device_ids=true | all-gather | bytes 36864 | tf_op jit(solution)/shard_map/all_gather | solution.py:78
  74.9 1.5 %fusion.3 = bf16[8,256]{1,0:T(8,128)(2,1)S(1)} fusion(bf16[8,1024,2]{1,0,2:T(8,128)(2,1)S(1)} %dot_general.37, bf16[2,1024,256]{2,1,0:T(8,128)(2,1)} %bitcast.75, bf16[8,256]{1,0:T(8,128)(2,1)S(1)} %copy-done.5), kind=kOutput, calls=%fused_computation.5 | convolution fusion | flops 8394752 | bytes 1089536 | tf_op jit(solution)/shard_map/ktsh,thc->ksc/dot_general | solution.py:81
  76.4 14.1 %all_gather.11 = bf16[8,2048]{1,0:T(8,128)(2,1)S(1)} all-gather(bf16[8,256]{1,0:T(8,128)(2,1)S(1)} %fusion.3), channel_id=1, replica_groups=mesh['grp'=2,'dp'=2,'kv'=4,'tp'=2] {'kv','tp'}, dimensions={1}, use_global_device_ids=true | all-gather | bytes 36864 | tf_op jit(solution)/shard_map/all_gather | solution.py:87
  90.5 0.1 fusion.4
  90.6 2.7 %fusion.32 = f32[8,704]{1,0:T(8,128)S(1)} fusion(bf16[2048,704]{0,1:T(8,128)(2,1)} %param.25, bf16[8,2048]{1,0:T(8,128)(2,1)S(1)} %all_gather.11, f32[2048]{0:T(1024)S(1)} %copy-done.3, f32[8]{0:T(128)S(1)} %add_rsqrt_fusion.1), kind=kOutput, calls=%fused_computation.50 | convolution fusion | flops 23134208 | bytes 2947104 | tf_op jit(solution)/shard_map/dot_general | solution.py:91
  93.3 4.1 %fusion.1 = f32[8,2048]{1,0:T(8,128)} fusion(bf16[704,2048]{1,0:T(8,128)(2,1)S(1)} %copy-done, bf16[2048,704]{0,1:T(8,128)(2,1)} %param.26, f32[8,704]{1,0:T(8,128)S(1)} %fusion.32, bf16[8,2048]{1,0:T(8,128)(2,1)S(1)} %all_gather.11, f32[2048]{0:T(1024)S(1)} %copy-done.3, f32[8]{0:T(128)S(1)} %add_rsqrt_fusion.1), kind=kOutput, calls=%fused_computation.2 | convolution fusion | flops 46236672 | bytes 5896224 | tf_op jit(solution)/shard_map/dot_general | solution.py:94
  97.4 30.7 %reduce-scatter.2.cloned.1.call-done = f32[8,256]{1,0:T(8,128)} async-done(((f32[8,2048]{1,0:T(8,128)}), f32[8,256]{1,0:T(8,128)}) %reduce-scatter.2.cloned.1.call-update) | async-done | bytes 8208 | tf_op jit(solution)/shard_map/reduce_scatter | solution.py:95
  128.2 1.3 add_convert_fusion
  (29 shorter events, 0.2 us)
Async XLA Ops:
  7.2 86.1 %copy-start = (bf16[704,2048]{1,0:T(8,128)(2,1)S(1)}, bf16[704,2048]{1,0:T(8,128)(2,1)}, u32[]{:S(2)}) copy-start(bf16[704,2048]{1,0:T(8,128)(2,1)} %param.27) | copy-start | bytes 8650756
  7.2 10.3 %copy-start.8 = (u32[32]{0:T(128)S(1)}, u32[32]{0:T(128)}, u32[]{:S(2)}) copy-start(u32[32]{0:T(128)} %constant.38) | copy-start | bytes 388
  7.2 9.3 %copy-start.4 = (f32[512]{0:T(512)S(1)}, f32[512]{0:T(512)}, u32[]{:S(2)}) copy-start(f32[512]{0:T(512)} %param.16) | copy-start | bytes 6148
  7.2 10.2 %copy-start.6 = (f32[1024]{0:T(1024)S(1)}, f32[1024]{0:T(1024)}, u32[]{:S(2)}) copy-start(f32[1024]{0:T(1024)} %param.21) | copy-start | bytes 12292
  7.2 47.9 %all-reduce.7.cloned.1.call-start = ((), (), s32[]{:S(2)}) async-start(), calls=%async_computation.2 | async-start | bytes 263168
  7.3 9.2 %copy-start.2 = (bf16[512,1024]{1,0:T(8,128)(2,1)S(1)}, bf16[512,1024]{1,0:T(8,128)(2,1)}, u32[]{:S(2)}) copy-start(bf16[512,1024]{1,0:T(8,128)(2,1)} %param.18) | copy-start | bytes 3145732
  14.3 46.4 %copy-start.7 = (f32[128]{0:T(128)S(1)}, f32[128]{0:T(128)}, u32[]{:S(2)}) copy-start(f32[128]{0:T(128)} %param.22) | copy-start | bytes 1540
  14.3 60.6 %copy-start.5 = (bf16[8,256]{1,0:T(8,128)(2,1)S(1)}, bf16[8,256]{1,0:T(8,128)(2,1)}, u32[]{:S(2)}) copy-start(bf16[8,256]{1,0:T(8,128)(2,1)} %param.14) | copy-start | bytes 12292
  16.5 74.2 %copy-start.3 = (f32[2048]{0:T(1024)S(1)}, f32[2048]{0:T(1024)}, u32[]{:S(2)}) copy-start(f32[2048]{0:T(1024)} %param.24) | copy-start | bytes 24580
  17.4 110.8 %reduce-scatter.2.cloned.1.call-start = ((), (), s32[]{:S(2)}) async-start(), calls=%async_computation.1 | async-start | bytes 73728 | tf_op jit(solution)/shard_map/reduce_scatter | solution.py:95
  58.6 1.0 copy-start.1
Sparse Core Ops, SparseCore 0:
  17.5 37.5 all-reduce.6
  97.6 30.5 reduce-scatter.1
where the time goes:
time: 137 us; the launch traced here: 136 us
  waiting for transfers between devices  67 us (49%)
  blocking collectives  30.4 us (22%)
  matrix products  16.4 us (12%)
  between operations  14.9 us (11%)
  other arithmetic  5.75 us (4%)
  local copies, waits for them, and re-layouts  1.73 us (1%)
    unnamed x3, waiting for transfers between devices  36.3 us
    reduce_scatter x1, waiting for transfers between devices, body(): lax.psum_scatter(terms, ('kv', 'tp'), scatter_dimension=1, tiled=True)  30.7 us
    all_gather x1, blocking collectives, body(): every_head = lax.all_gather(mixed, ('kv', 'tp'), axis=0, tiled=True)  14.1 us
    all_gather x1, blocking collectives, body(): gathered = lax.all_gather(middle, ('kv', 'tp'), axis=1, tiled=True)  14.1 us
    dot_general x1, matrix products, body(): terms = jnp.dot(hidden, w_down, preferred_element_type=jnp.float32)  4.12 us
  transfers between devices with their start and end apart: 2, of which 2 were waited for; matrix products, arithmetic and copies ran while one was open for 0% of the time, Pallas kernels for 0%

commit v1 on v0

--- a/solution.py
+++ b/solution.py
@@ -84,7 +84,15 @@
     middle = (
         tokens.astype(jnp.float32) + projected.reshape(kv_count * rows_local, width_cols)
     ).astype(jnp.bfloat16)
-    gathered = lax.all_gather(middle, ("kv", "tp"), axis=1, tiled=True)
+
+    def store_spot_up(local_x, along_axis):
+        z = jnp.stack(tuple((local_x for _ in range(lax.axis_size(along_axis)))), axis=0)
+        h_now = jnp.concatenate(
+            lax.all_to_all(z, axis_name=along_axis, split_axis=0, concat_axis=0), 1
+        )
+        return h_now
+
+    gathered = store_spot_up(middle, ("kv", "tp"))
     gathered_f = gathered.astype(jnp.float32)
     mlp_scale = lax.rsqrt(jnp.mean(gathered_f * gathered_f, axis=1, keepdims=True) + epsilon)
     mlp_in = (gathered_f * mlp_scale * mlp_gain).astype(jnp.bfloat16)

time: 137 us -> 130 us (0.949)
  blocking collectives: 30.4 us -> 25.6 us
  waiting for transfers between devices: 67 us -> 65.2 us
    all_gather x1 -> x0, blocking collectives: 14.1 us -> none  [body(): gathered = lax.all_gather(middle, ('kv', 'tp'), axis=1, tiled=True)]
    all_to_all x0 -> x1, blocking collectives: none -> 9.25 us  [store_spot_up(): lax.all_to_all(z, axis_name=along_axis, split_axis=0, concat_axis=0)]
    reduce_scatter x1, waiting for transfers between devices: 30.7 us -> 28.9 us  [body(): lax.psum_scatter(terms, ('kv', 'tp'), scatter_dimension=1, tiled=True)]
  transfers between devices with their start and end apart: 2 -> 2, of which waited for: 2 -> 2; matrix products, arithmetic and copies ran while one was open for 0% -> 1% of each run, Pallas kernels for 0% -> 0%
where the time goes in v1:
time: 130 us
  waiting for transfers between devices  65.2 us (50%)
  blocking collectives  25.6 us (20%)
  matrix products  16.4 us (13%)
  between operations  14.9 us (11%)
  other arithmetic  5.75 us (4%)
  local copies, waits for them, and re-layouts  1.74 us (1%)
    unnamed x3, waiting for transfers between devices  36.3 us
    reduce_scatter x1, waiting for transfers between devices, body(): lax.psum_scatter(terms, ('kv', 'tp'), scatter_dimension=1, tiled=True)  28.9 us
    all_gather x1, blocking collectives, body(): every_head = lax.all_gather(mixed, ('kv', 'tp'), axis=0, tiled=True)  14.1 us
    all_to_all x1, blocking collectives, store_spot_up(): lax.all_to_all(z, axis_name=along_axis, split_axis=0, concat_axis=0)  9.25 us
    dot_general x1, matrix products, body(): terms = jnp.dot(hidden, w_down, preferred_element_type=jnp.float32)  4.12 us
    dot_general x1, matrix products, body(): gate = jnp.dot(mlp_in, w_gate, preferred_element_type=jnp.float32)  2.66 us
  transfers between devices with their start and end apart: 2, of which 2 were waited for; matrix products, arithmetic and copies ran while one was open for 1% of the time, Pallas kernels for 0%

profile of v1, /device:TPU:0, one launch (start us, length us, event | category | flops | bytes accessed | tf_op | source)
XLA Modules:
  0.0 129.7 jit_solution(3326342565466569730)
XLA Ops:
  7.3 2.2 %all_gather.6 = bf16[8,512]{1,0:T(8,128)(2,1)S(1)} all-gather(bf16[8,256]{1,0:T(8,128)(2,1)} %param.14), channel_id=1, replica_groups=mesh['grp'=2,'dp'=2,'kv'=4,'tp'=2] {'tp'}, dimensions={1}, use_global_device_ids=true | all-gather | bytes 12288 | tf_op jit(solution)/shard_map/all_gather | solution.py:33
  9.5 0.6 fusion.10
  10.1 2.1 %fusion.31 = f32[8,1024]{1,0:T(8,128)} fusion(bf16[512,1024]{1,0:T(8,128)(2,1)} %param.19, bf16[8,512]{1,0:T(8,128)(2,1)S(1)} %all_gather.6, f32[512]{0:T(512)} %param.16), kind=kOutput, calls=%fused_computation.51 | convolution fusion | flops 8400896 | bytes 1091584 | tf_op jit(solution)/shard_map/dot_general | solution.py:53
  12.2 2.1 %fusion.29 = f32[8,1024]{1,0:T(8,128)} fusion(bf16[512,1024]{1,0:T(8,128)(2,1)} %param.17, bf16[8,512]{1,0:T(8,128)(2,1)S(1)} %all_gather.6, f32[512]{0:T(512)} %param.16), kind=kOutput, calls=%fused_computation.50 | convolution fusion | flops 8400896 | bytes 1091584 | tf_op jit(solution)/shard_map/dot_general | solution.py:41
  14.3 2.1 %fusion.27 = f32[8,1024]{1,0:T(8,128)} fusion(bf16[512,1024]{1,0:T(8,128)(2,1)} %param.20, bf16[8,512]{1,0:T(8,128)(2,1)S(1)} %all_gather.6, f32[512]{0:T(512)} %param.16), kind=kOutput, calls=%fused_computation.49 | convolution fusion | flops 8400896 | bytes 1091584 | tf_op jit(solution)/shard_map/dot_general | solution.py:59
  16.5 0.9 fusion.33
  17.4 0.0 reduce-scatter.2.cloned.1.call-start
  17.5 0.7 dynamic-slice
  18.8 36.2 %all-reduce.7.cloned.1.call-done = (f32[8,1024]{1,0:T(8,128)}, f32[8]{0:T(128)}, f32[8,1024]{1,0:T(8,128)}, f32[8,1024]{1,0:T(8,128)}, f32[8,1024]{1,0:T(8,128)}) async-done(((f32[8,1024]{1,0:T(8,128)}, f32[8]{0:T(128)}, f32[8,1024]{1,0:T(8,128)}, f32[8,1024]{1,0:T(8,128)}, f32[8,1024]{1,0:T(8,128)}), (f32[8,1024]{1,0:T(8,128)}, f32[8]{0:T(128)}, f32[8,1024]{1,0:T(8,128)}, f32[8,1024]{1,0:T(8,128)}, ...) | async-done | bytes 131120
  55.1 0.8 add_rsqrt_fusion.2
  55.8 0.9 fusion.21
  56.8 1.8 %multiply_add_fusion = f32[2,8,128,128]{3,2,1,0:T(8,128)S(1)} fusion(f32[2,8,128,128]{3,2,1,0:T(8,128)} %param.15, f32[2,8,128]{2,1,0:T(8,128)S(1)} %bitcast.84, f32[2,8,128]{2,1,0:T(8,128)S(1)} %get-tuple-element.7, f32[2,8,128]{2,1,0:T(8,128)S(1)} %get-tuple-element.8), kind=kLoop, calls=%fused_computation.6 | loop fusion | flops 786432 | bytes 2121728 | tf_op jit(solution)/shard_map/add | solution.py:72
  58.6 1.0 copy-done.1
  59.6 1.0 fusion.38
  60.6 0.1 multiply_reduce_fusion.1
  60.7 0.1 fusion.26
  60.8 14.1 %all_gather.7 = bf16[8,2,1024]{2,1,0:T(2,128)(2,1)S(1)} all-gather(bf16[1,2,1024]{2,1,0:T(2,128)(2,1)S(1)} %convert_element_type.56), channel_id=1, replica_groups=mesh['grp'=2,'dp'=2,'kv'=4,'tp'=2] {'kv','tp'}, dimensions={0}, use_global_device_ids=true | all-gather | bytes 36864 | tf_op jit(solution)/shard_map/all_gather | solution.py:78
  74.9 1.5 %fusion.3 = bf16[8,256]{1,0:T(8,128)(2,1)S(1)} fusion(bf16[8,1024,2]{1,0,2:T(8,128)(2,1)S(1)} %dot_general.37, bf16[2,1024,256]{2,1,0:T(8,128)(2,1)} %bitcast.78, bf16[8,256]{1,0:T(8,128)(2,1)S(1)} %copy-done.5), kind=kOutput, calls=%fused_computation.5 | convolution fusion | flops 8394752 | bytes 1089536 | tf_op jit(solution)/shard_map/ktsh,thc->ksc/dot_general | solution.py:81
  76.4 9.3 %all_to_all.5 = bf16[8,8,256]{2,1,0:T(8,128)(2,1)S(1)} all-to-all(bf16[8,8,256]{2,1,0:T(8,128)(2,1)S(1)} %stack.2), channel_id=1, replica_groups=mesh['grp'=2,'dp'=2,'kv'=4,'tp'=2] {'kv','tp'}, dimensions={0} | all-to-all | bytes 65536 | tf_op jit(solution)/shard_map/all_to_all | solution.py:91
  85.7 0.1 multiply_reduce_fusion
  85.8 2.7 %fusion.36 = f32[8,704]{1,0:T(8,128)S(1)} fusion(bf16[2048,704]{0,1:T(8,128)(2,1)} %param.25, f32[8,2048]{1,0:T(8,128)S(1)} %bitcast.79, f32[2048]{0:T(1024)S(1)} %copy-done.3, f32[8]{0:T(128)S(1)} %add_rsqrt_fusion.1), kind=kOutput, calls=%fused_computation.58 | convolution fusion | flops 23117824 | bytes 2979872 | tf_op jit(solution)/shard_map/dot_general | solution.py:99
  88.5 4.1 %fusion.1 = f32[8,2048]{1,0:T(8,128)} fusion(bf16[704,2048]{1,0:T(8,128)(2,1)S(1)} %copy-done, bf16[2048,704]{0,1:T(8,128)(2,1)} %param.26, f32[8,704]{1,0:T(8,128)S(1)} %fusion.36, f32[8,2048]{1,0:T(8,128)S(1)} %bitcast.80, f32[2048]{0:T(1024)S(1)} %copy-done.3, f32[8]{0:T(128)S(1)} %add_rsqrt_fusion.1), kind=kOutput, calls=%fused_computation.2 | convolution fusion | flops 46220288 | bytes 5928992 | tf_op jit(solution)/shard_map/dot_general | solution.py:102
  92.6 28.9 %reduce-scatter.2.cloned.1.call-done = f32[8,256]{1,0:T(8,128)} async-done(((f32[8,2048]{1,0:T(8,128)}), f32[8,256]{1,0:T(8,128)}) %reduce-scatter.2.cloned.1.call-update) | async-done | bytes 8208 | tf_op jit(solution)/shard_map/reduce_scatter | solution.py:103
  121.6 1.3 add_convert_fusion
  (31 shorter events, 0.2 us)
Async XLA Ops:
  7.2 81.3 %copy-start = (bf16[704,2048]{1,0:T(8,128)(2,1)S(1)}, bf16[704,2048]{1,0:T(8,128)(2,1)}, u32[]{:S(2)}) copy-start(bf16[704,2048]{1,0:T(8,128)(2,1)} %param.27) | copy-start | bytes 8650756
  7.2 10.3 %copy-start.8 = (u32[32]{0:T(128)S(1)}, u32[32]{0:T(128)}, u32[]{:S(2)}) copy-start(u32[32]{0:T(128)} %constant.38) | copy-start | bytes 388
  7.2 9.3 %copy-start.4 = (f32[512]{0:T(512)S(1)}, f32[512]{0:T(512)}, u32[]{:S(2)}) copy-start(f32[512]{0:T(512)} %param.16) | copy-start | bytes 6148
  7.2 10.2 %copy-start.6 = (f32[1024]{0:T(1024)S(1)}, f32[1024]{0:T(1024)}, u32[]{:S(2)}) copy-start(f32[1024]{0:T(1024)} %param.21) | copy-start | bytes 12292
  7.2 47.9 %all-reduce.7.cloned.1.call-start = ((), (), s32[]{:S(2)}) async-start(), calls=%async_computation.3 | async-start | bytes 263168
  7.3 9.2 %copy-start.2 = (bf16[512,1024]{1,0:T(8,128)(2,1)S(1)}, bf16[512,1024]{1,0:T(8,128)(2,1)}, u32[]{:S(2)}) copy-start(bf16[512,1024]{1,0:T(8,128)(2,1)} %param.18) | copy-start | bytes 3145732
  14.3 46.4 %copy-start.7 = (f32[128]{0:T(128)S(1)}, f32[128]{0:T(128)}, u32[]{:S(2)}) copy-start(f32[128]{0:T(128)} %param.22) | copy-start | bytes 1540
  14.3 60.6 %copy-start.5 = (bf16[8,256]{1,0:T(8,128)(2,1)S(1)}, bf16[8,256]{1,0:T(8,128)(2,1)}, u32[]{:S(2)}) copy-start(bf16[8,256]{1,0:T(8,128)(2,1)} %param.14) | copy-start | bytes 12292
  16.5 69.4 %copy-start.3 = (f32[2048]{0:T(1024)S(1)}, f32[2048]{0:T(1024)}, u32[]{:S(2)}) copy-start(f32[2048]{0:T(1024)} %param.24) | copy-start | bytes 24580
  17.4 104.2 %reduce-scatter.2.cloned.1.call-start = ((), (), s32[]{:S(2)}) async-start(), calls=%async_computation.2 | async-start | bytes 73728 | tf_op jit(solution)/shard_map/reduce_scatter | solution.py:103
  58.6 1.0 copy-start.1
Sparse Core Ops, SparseCore 0:
  17.5 37.5 all-reduce.6
  92.8 28.7 reduce-scatter.1
